TPU v7x, 32 devices: a whole 2x2x4 slice. The times are simulated.
32 devices in a mesh: grp: 2 (over y), ep: 4 (over z), tp: 4 (over x, core).
Axes of the slice: x: 2, y: 2, z: 4, core: 2. Of those that a mesh axis runs over, the one named last changes fastest.
Arguments:
- tokens: bfloat16 [512, 4096], P(('grp', 'ep'), 'tp'), parts along dimension 0, may hold values from -27 to 27
- group_choice: int32 [512], P(('grp', 'ep')), parts along dimension 0, may hold values from 0 to 1, as said below
- member_choice: int32 [512, 2], P(('grp', 'ep')), parts along dimension 0, may hold values from 0 to 1, as said below
- group_prob: float32 [512], P(('grp', 'ep')), parts along dimension 0, may hold values from 0.3 to 1
- member_score: float32 [512, 2], P(('grp', 'ep')), parts along dimension 0, may hold values from -4 to 4
- norm_gain: float32 [4096], P('tp'), may hold values from 0.1 to 1.9
- w_gate: bfloat16 [4, 4096, 1024], P('ep', 'tp'), may hold values from -0.09375 to 0.09375
- w_up: bfloat16 [4, 4096, 1024], P('ep', 'tp'), may hold values from -0.09375 to 0.09375
- w_down: bfloat16 [4, 1024, 4096], P('ep', None, 'tp'), may hold values from -0.1875 to 0.1875
- final_gain: float32 [4096], P('tp'), may hold values from 0.1 to 1.9
Outputs:
- mixed: bfloat16 [512, 4096], P(('grp', 'ep'), 'tp'), parts along dimension 0
There are 2 independent parts, one for each index of `grp`. A program takes and returns all parts, laid end to end along the dimension named above; an argument that names none is the same for every part. Nothing has to cross between parts.
Inputs may be any that keep to these rules, and one draw needn't show every extreme that they name: `group_choice`: in each aligned block of 64 tokens every group is chosen by exactly 32 tokens. `member_choice`: each row names 2 different experts of its token's group. In each aligned block of 64 rows no expert (group and member together) is named by more than 32 rows, some expert is named by exactly 32 rows, and one expert is named by exactly 32 rows in every block.
All inputs are finite; a program needn't handle non-finite values.
Results may differ from a plain program's by a relative error of at most 0.017.
Values may be sent and summed in bfloat16 or wider, within the bound.
A program may use at most 64 MiB of HBM per device.

v0:
```python
import functools

import jax
import jax.numpy as jnp
from jax import lax
from jax.experimental import pallas as pl
from jax.experimental.pallas import tpu as pltpu
from jax.sharding import PartitionSpec as P

EPS = 1e-06
MESH = pl.DeviceIdType.MESH
F32 = jnp.float32
BF16 = jnp.bfloat16
PLAN = (
    ("a", 0), ("a", 1), ("b", 0), ("a", 2), ("a", 3), ("b", 1),
    ("c", 0), ("b", 2), ("b", 3), ("c", 2), ("c", 1), ("c", 3),
)
VMEM_LIMIT = 56 * 2**20


def partner(me, s, n):
    out, bit = me, 1
    while bit < n:
        if s & bit:
            out = out + bit - 2 * bit * ((me // bit) % 2)
        bit *= 2
    return out


def iota(shape, dim):
    return lax.broadcasted_iota(jnp.int32, shape, dim)


def to_row(col, width):
    n = col.shape[0]
    eye = iota((n, width), 0) == iota((n, width), 1)
    return jnp.sum(jnp.where(eye, col, 0.0), axis=0, keepdims=True)


def to_col(row, n):
    width = row.shape[1]
    eye = iota((n, width), 0) == iota((n, width), 1)
    return jnp.sum(jnp.where(eye, row, 0.0), axis=1, keepdims=True)


def kernel(
    cfg,
    x_hbm,
    group_hbm,
    member_hbm,
    prob_hbm,
    score_hbm,
    ngain_hbm,
    wg_hbm,
    wu_hbm,
    wd_hbm,
    out_ref,
    x_ref,
    group_ref,
    member_ref,
    prob_ref,
    score_ref,
    ngain_ref,
    wg,
    wu,
    wd,
    xs,
    xr,
    ps,
    pr,
    sqs,
    sqr,
    hs,
    hr,
    ob,
    ret,
    fs,
    fr,
    w_sem,
    x_send,
    x_recv,
    p_send,
    p_recv,
    q_send,
    q_recv,
    h_send,
    h_recv,
    o_send,
    o_recv,
    f_send,
    f_recv,
):
    n_ep, n_tp, groups, order, chunks = cfg
    per_group = n_ep // groups
    tok, dim = x_ref.shape
    cap = tok // groups
    ff = wg.shape[1]
    q = ff // n_tp
    full_width = dim * n_tp
    me_e = lax.axis_index("ep")
    me_t = lax.axis_index("tp")

    barrier = pltpu.get_barrier_semaphore()
    for s in range(1, n_ep):
        pl.semaphore_signal(barrier, inc=1, device_id={"ep": partner(me_e, s, n_ep)}, device_id_type=MESH)
    for s in range(1, n_tp):
        pl.semaphore_signal(barrier, inc=1, device_id={"tp": partner(me_t, s, n_tp)}, device_id_type=MESH)

    moves = (
        (group_hbm, group_ref),
        (x_hbm, x_ref),
        (ngain_hbm, ngain_ref),
        (wg_hbm.at[0], wg),
        (wu_hbm.at[0], wu),
        (member_hbm, member_ref),
        (prob_hbm, prob_ref),
        (score_hbm, score_ref),
        (wd_hbm.at[0], wd),
    )
    loads = [pltpu.make_async_copy(src, dst, w_sem.at[i]) for i, (src, dst) in enumerate(moves)]
    for load in loads:
        load.start()
    loads[0].wait()
    loads[1].wait()

    group_row = group_ref[...]
    rows8 = max(8, groups)
    onehot = (iota((rows8, tok), 0) == group_row).astype(F32)
    strict = (iota((tok, tok), 0) < iota((tok, tok), 1)).astype(F32)
    rank = jnp.dot(onehot.astype(BF16), strict.astype(BF16), preferred_element_type=F32)
    slot_row = jnp.sum(
        onehot * (iota((rows8, tok), 0).astype(F32) * cap + rank), axis=0, keepdims=True
    )
    picker = (iota((tok, tok), 0).astype(F32) == slot_row).astype(BF16)
    x = x_ref[...]
    xs[...] = jnp.dot(picker, x, preferred_element_type=F32).astype(BF16)

    pending = []

    def send(src, dst, ssem, rsem, where):
        copy = pltpu.make_async_remote_copy(
            src_ref=src, dst_ref=dst, send_sem=ssem, recv_sem=rsem, device_id=where, device_id_type=MESH
        )
        copy.start()
        pending.append(copy)
        return copy

    def group_rows(e):
        return pl.ds(pl.multiple_of((e // per_group) * cap, cap), cap)

    xr[pl.ds(0, cap), :] = xs[group_rows(me_e), :]
    x_copies = {}

    def dispatch():
        for k in range(1, n_ep):
            e = partner(me_e, order[k], n_ep)
            x_copies[k] = send(
                xs.at[group_rows(e)], xr.at[pl.ds(k * cap, cap)], x_send.at[k], x_recv.at[k], {"ep": e}
            )

    loads[2].wait()
    ngain = ngain_ref[...]
    tp_order = [s for s in range(2, n_tp)] + [s for s in range(1, min(2, n_tp))]
    p_copies, q_copies, h_copies, o_copies = {}, {}, {}, {}
    own_sq = {}

    def span(c):
        first, count = chunks[c]
        return first * cap, count * cap

    def products(c):
        start, rows = span(c)
        vals = xr[pl.ds(start, rows), :].astype(F32)
        sq = jnp.sum(vals * vals, axis=1, keepdims=True)
        own_sq[c] = sq
        width = sqs.shape[2]
        sqs[c] = jnp.broadcast_to(to_row(sq, width), (8, width))
        rows_in = (vals * ngain).astype(BF16)
        for s in tp_order + [0]:
            p = partner(me_t, s, n_tp)
            cols = pl.ds(pl.multiple_of(p * q, q), q)
            ps[s, pl.ds(start, rows), pl.ds(0, q)] = jnp.dot(
                rows_in, wg[:, cols], preferred_element_type=F32
            ).astype(BF16)
            ps[s, pl.ds(start, rows), pl.ds(q, q)] = jnp.dot(
                rows_in, wu[:, cols], preferred_element_type=F32
            ).astype(BF16)
            if s > 0:
                send_part(c, s)

    def send_part(c, s):
        start, rows = span(c)
        peer = {"tp": partner(me_t, s, n_tp)}
        p_copies[c, s] = send(
            ps.at[s, pl.ds(start, rows)],
            pr.at[s, pl.ds(start, rows)],
            p_send.at[c, s],
            p_recv.at[c, s],
            peer,
        )
        q_copies[c, s] = send(sqs.at[c], sqr.at[c, s], q_send.at[c, s], q_recv.at[c, s], peer)

    def stage_a(c):
        first, count = chunks[c]
        for k in range(max(first, 1), first + count):
            x_copies[k].wait_recv()
        products(c)

    def stage_b(c):
        start, rows = span(c)
        total = own_sq[c]
        for s in range(1, n_tp):
            q_copies[c, s].wait_recv()
            total = total + to_col(sqr[c, s][0:1, :], rows)
        scale = lax.rsqrt(total / full_width + EPS)
        g = ps[0, pl.ds(start, rows), pl.ds(0, q)].astype(F32)
        u = ps[0, pl.ds(start, rows), pl.ds(q, q)].astype(F32)
        for s in range(1, n_tp):
            p_copies[c, s].wait_recv()
            g = g + pr[s, pl.ds(start, rows), pl.ds(0, q)].astype(F32)
            u = u + pr[s, pl.ds(start, rows), pl.ds(q, q)].astype(F32)
        g, u = g * scale, u * scale
        hidden = (g / (1.0 + jnp.exp(-g)) * u).astype(BF16)
        hs[pl.ds(start, rows), :] = hidden
        for s in tp_order:
            h_copies[c, s] = send(
                hs.at[pl.ds(start, rows)],
                hr.at[s, pl.ds(start, rows)],
                h_send.at[c, s],
                h_recv.at[c, s],
                {"tp": partner(me_t, s, n_tp)},
            )

    def stage_c(c):
        first, count = chunks[c]
        start, rows = span(c)
        if c == 0:
            loads[8].wait()
        acc = None
        for s in range(n_tp):
            if s > 0:
                h_copies[c, s].wait_recv()
                h = hr[s, pl.ds(start, rows), :]
            else:
                h = hs[pl.ds(start, rows), :]
            p = partner(me_t, s, n_tp)
            term = jnp.dot(h, wd[pl.ds(pl.multiple_of(p * q, q), q), :], preferred_element_type=F32)
            acc = term if acc is None else acc + term
        ob[pl.ds(start, rows), :] = acc.astype(BF16)
        for k in range(first, first + count):
            if k > 0:
                o_copies[k] = send(
                    ob.at[pl.ds(k * cap, cap)],
                    ret.at[pl.ds(k * cap, cap)],
                    o_send.at[k],
                    o_recv.at[k],
                    {"ep": partner(me_e, order[k], n_ep)},
                )

    pl.semaphore_wait(barrier, n_ep - 1 + n_tp - 1)
    dispatch()
    loads[3].wait()
    loads[4].wait()
    stage_a(0)
    for load in loads[5:8]:
        load.wait()
    scores = jnp.exp(score_ref[...])
    weights = prob_ref[...] * scores / jnp.sum(scores, axis=0, keepdims=True)
    slot_col = to_col(slot_row, tok).astype(jnp.int32)
    ids = group_row * per_group + member_ref[...]
    expert_cols = []
    for k in range(n_ep):
        named = jnp.where(ids == partner(me_e, order[k], n_ep), weights, 0.0)
        expert_cols.append(to_col(jnp.sum(named, axis=0, keepdims=True), tok))

    stages = {"a": stage_a, "b": stage_b, "c": stage_c}
    for stage, c in PLAN[1:]:
        stages[stage](c)

    summed = x.astype(F32)
    for k in range(n_ep):
        e = partner(me_e, order[k], n_ep)
        if k > 0:
            o_copies[k].wait_recv()
            rows = ret[pl.ds(k * cap, cap), :]
        else:
            rows = ob[pl.ds(0, cap), :]
        pick = (iota((tok, cap), 1) + (e // per_group) * cap == slot_col).astype(F32).astype(BF16)
        summed = summed + expert_cols[k] * jnp.dot(pick, rows, preferred_element_type=F32)

    square = jnp.sum(summed * summed, axis=1, keepdims=True)
    width = fs.shape[1]
    fs[...] = jnp.broadcast_to(to_row(square, width), (8, width))
    f_copies = {}
    for s in tp_order:
        f_copies[s] = send(fs, fr.at[s], f_send.at[s], f_recv.at[s], {"tp": partner(me_t, s, n_tp)})
    for s in range(1, n_tp):
        f_copies[s].wait_recv()
        square = square + to_col(fr[s][0:1, :], tok)
    out_ref[...] = summed * lax.rsqrt(square / full_width + EPS)

    for copy in pending:
        copy.wait_send()


def solution(mesh):
    n_ep, n_tp = mesh.shape["ep"], mesh.shape["tp"]
    groups = max(2, n_ep // 8)
    order = range(n_ep)
    n_chunks = 4
    each = n_ep // n_chunks
    chunks = tuple((i * each, each) for i in range(n_chunks))

    def local(tokens, group_choice, member_choice, group_prob, member_score, norm_gain, w_gate, w_up, w_down, final_gain):
        tok, dim = tokens.shape
        ff, top = w_gate.shape[2], member_choice.shape[1]
        cap = tok // groups
        q = ff // n_tp
        all_rows = n_ep * cap
        width = -(-max(count * cap for _, count in chunks) // 128) * 128
        out_width = -(-tok // 128) * 128
        vmem = pl.BlockSpec(memory_space=pltpu.VMEM)
        hbm = pl.BlockSpec(memory_space=pltpu.HBM)
        dma = pltpu.SemaphoreType.DMA
        nc = len(chunks)
        normal = pl.pallas_call(
            functools.partial(kernel, (n_ep, n_tp, groups, tuple(order), chunks)),
            out_shape=pltpu.VMEM((tok, dim), F32),
            in_specs=[hbm] * 9,
            out_specs=vmem,
            scratch_shapes=[
                pltpu.VMEM((tok, dim), BF16),
                pltpu.VMEM((1, tok), jnp.int32),
                pltpu.VMEM((top, tok), jnp.int32),
                pltpu.VMEM((1, tok), F32),
                pltpu.VMEM((top, tok), F32),
                pltpu.VMEM((1, dim), F32),
                pltpu.VMEM((dim, ff), BF16),
                pltpu.VMEM((dim, ff), BF16),
                pltpu.VMEM((ff, dim), BF16),
                pltpu.VMEM((tok, dim), BF16),
                pltpu.VMEM((all_rows, dim), BF16),
                pltpu.VMEM((n_tp, all_rows, 2 * q), BF16),
                pltpu.VMEM((n_tp, all_rows, 2 * q), BF16),
                pltpu.VMEM((nc, 8, width), F32),
                pltpu.VMEM((nc, n_tp, 8, width), F32),
                pltpu.VMEM((all_rows, q), BF16),
                pltpu.VMEM((n_tp, all_rows, q), BF16),
                pltpu.VMEM((all_rows, dim), BF16),
                pltpu.VMEM((all_rows, dim), BF16),
                pltpu.VMEM((8, out_width), F32),
                pltpu.VMEM((n_tp, 8, out_width), F32),
                dma((9,)),
                dma((n_ep,)),
                dma((n_ep,)),
                dma((nc, n_tp)),
                dma((nc, n_tp)),
                dma((nc, n_tp)),
                dma((nc, n_tp)),
                dma((nc, n_tp)),
                dma((nc, n_tp)),
                dma((n_ep,)),
                dma((n_ep,)),
                dma((n_tp,)),
                dma((n_tp,)),
            ],
            compiler_params=pltpu.CompilerParams(collective_id=0, has_side_effects=True, vmem_limit_bytes=VMEM_LIMIT),
        )(
            tokens,
            group_choice.reshape(1, tok),
            member_choice.T,
            group_prob.reshape(1, tok),
            member_score.T,
            norm_gain.reshape(1, dim),
            w_gate,
            w_up,
            w_down,
        )
        return (normal * final_gain[None, :]).astype(BF16)

    return jax.shard_map(
        local,
        mesh=mesh,
        in_specs=(
            P(("grp", "ep"), "tp"),
            P(("grp", "ep")),
            P(("grp", "ep"), None),
            P(("grp", "ep")),
            P(("grp", "ep"), None),
            P("tp"),
            P("ep", "tp", None),
            P("ep", "tp", None),
            P("ep", None, "tp"),
            P("tp"),
        ),
        out_specs=P(("grp", "ep"), "tp"),
        check_vma=False,
    )
```

profile of v0, /device:TPU:0, one launch (start us, length us, event | category | flops | bytes accessed | tf_op | source)
XLA Modules:
  0.0 30.1 jit_solution(14172527165361611998)
XLA Ops:
  0.0 0.0 copy-start
  0.0 29.4 %shard_map.100 = f32[64,1024]{1,0:T(8,128)S(1)} custom-call(bf16[64,1024]{1,0:T(8,128)(2,1)} %x_hbm.1, s32[1,64]{1,0:T(1,128)} %bitcast.8, s32[2,64]{1,0:T(2,128)} %bitcast.6, f32[1,64]{1,0:T(1,128)} %bitcast.9, f32[2,64]{1,0:T(2,128)} %bitcast.7, f32[1,1024]{1,0:T(1,128)} %bitcast.5, bf16[1,1024,1024]{2,1,0:T(8,128)(2,1)} %wg_hbm.1, ...), custom_call_target="tpu_custom_call" | custom-call | tf_op jit(solution)/shard_map/pallas_call | solution.py:326
  29.4 0.0 copy-done
  29.4 0.7 %multiply_convert_fusion = bf16[64,1024]{1,0:T(8,128)(2,1)} fusion(f32[64,1024]{1,0:T(8,128)S(1)} %shard_map.100, f32[1024]{0:T(1024)S(1)} %copy-done), kind=kLoop, calls=%fused_computation | loop fusion | flops 131072 | bytes 397312 | tf_op jit(solution)/shard_map/convert_element_type | solution.py:379
Async XLA Ops:
  0.0 29.4 %copy-start = (f32[1024]{0:T(1024)S(1)}, f32[1024]{0:T(1024)}, u32[]{:S(2)}) copy-start(f32[1024]{0:T(1024)} %param.19) | copy-start | bytes 12292
where the time goes:
time: 30.3 us; the launch traced here: 30.1 us
  Pallas kernels  29.4 us (97%)
  other arithmetic  0.67 us (2%)
    pallas_call x1, Pallas kernels, local(): pl.pallas_call(functools.partial(kernel, (n_ep, n_tp, groups, tuple(order...  29.4 us
    convert_element_type x1, other arithmetic, local(): return (normal * final_gain[None, :]).astype(BF16)  0.67 us

commit v1 on v0

v1 whole, which is shorter than its diff:
```python
import functools

import jax
import jax.numpy as jnp
from jax import lax
from jax.experimental import pallas as pl
from jax.experimental.pallas import tpu as pltpu
from jax.sharding import PartitionSpec as P

EPS = 1e-06
MESH = pl.DeviceIdType.MESH
F32 = jnp.float32
BF16 = jnp.bfloat16
SEND = ((1, 2, 3), (3, 1, 2), (3, 1, 2), (1, 2, 3))
TAKE = ((1, 2, 3), (1, 3, 2), (3, 2, 1), (1, 3, 2))
BACK = (2, 3, 1)
AT_ONCE = 2
PLAN = (
    ("b", 0), ("a", 1), ("b", 1), ("a", 2), ("s", 0), ("b", 2), ("a", 3),
    ("c", 0), ("b", 3), ("s", 1), ("c", 1), ("s", 2), ("c", 2), ("s", 3), ("c", 3),
)
LANES = 128
CHUNKS = 4
VMEM_LIMIT = 56 * 2**20


def partner(me, s, n):
    out, bit = me, 1
    while bit < n:
        if s & bit:
            out = out + bit - 2 * bit * ((me // bit) % 2)
        bit *= 2
    return out


def parity(me, n):
    out, bit = 0, 1
    while bit < n:
        out = out + (me // bit) % 2
        bit *= 2
    return out % 2


def iota(shape, dim):
    return lax.broadcasted_iota(jnp.int32, shape, dim)


def to_row(col, width):
    n = col.shape[0]
    eye = iota((n, width), 0) == iota((n, width), 1)
    return jnp.sum(jnp.where(eye, col, 0.0), axis=0, keepdims=True)


def to_col(row, n):
    width = row.shape[1]
    eye = iota((n, width), 0) == iota((n, width), 1)
    return jnp.sum(jnp.where(eye, row, 0.0), axis=1, keepdims=True)


def pack(col):
    high = col.astype(BF16).astype(F32)
    middle = (col - high).astype(BF16).astype(F32)
    low = col - high - middle
    lane = iota((col.shape[0], LANES), 1)
    parts = jnp.where(lane == 0, high, jnp.where(lane == 1, middle, jnp.where(lane == 2, low, 0.0)))
    return parts.astype(BF16)


def unpack(parts):
    return jnp.sum(parts.astype(F32), axis=1, keepdims=True)


def kernel(
    cfg,
    x_hbm,
    group_hbm,
    member_hbm,
    prob_hbm,
    score_hbm,
    ngain_hbm,
    wg_hbm,
    wu_hbm,
    wd_hbm,
    out_ref,
    x_ref,
    group_ref,
    member_ref,
    prob_ref,
    score_ref,
    ngain_ref,
    wg,
    wu,
    wd,
    xs,
    xr,
    ps,
    pr,
    own,
    cs,
    cr,
    hs,
    hr,
    ob,
    ret,
    fs,
    fr,
    w_sem,
    send_sem,
    x_recv,
    p_recv,
    c_recv,
    h_recv,
    o_recv,
    f_recv,
):
    n_ep, n_tp, groups = cfg
    per_group = n_ep // groups
    tok, dim = x_ref.shape
    cap = tok // groups
    half = wg.shape[1] // 2
    full_width = dim * n_tp
    me_e = lax.axis_index("ep")
    me_t = lax.axis_index("tp")
    side = parity(me_t, n_tp)
    far = [s for s in range(1, n_tp) if parity(s, n_tp) == 0]
    each = n_ep // CHUNKS
    quarter = me_e // each

    def by_quarter(values):
        low, high = quarter % 2, quarter // 2
        return sum(
            v * (low if i % 2 else 1 - low) * (high if i // 2 else 1 - high) for i, v in enumerate(values)
        )

    def route(table, c, j):
        step = [0] * CHUNKS if c == 0 else [row[c - 1] for row in table]
        to = by_quarter([i ^ v for i, v in enumerate(step)]) * each + partner(me_e % each, j, each)
        return by_quarter(step) * each + j, to

    barrier = pltpu.get_barrier_semaphore()
    for s in range(1, n_ep):
        pl.semaphore_signal(barrier, inc=1, device_id={"ep": partner(me_e, s, n_ep)}, device_id_type=MESH)
    for s in range(1, n_tp):
        pl.semaphore_signal(barrier, inc=1, device_id={"tp": partner(me_t, s, n_tp)}, device_id_type=MESH)

    moves = (
        (group_hbm, group_ref),
        (x_hbm, x_ref),
        (ngain_hbm, ngain_ref),
        (wg_hbm.at[0], wg),
        (wu_hbm.at[0], wu),
        (member_hbm, member_ref),
        (prob_hbm, prob_ref),
        (score_hbm, score_ref),
        (wd_hbm.at[0], wd),
    )
    loads = [pltpu.make_async_copy(src, dst, w_sem.at[i]) for i, (src, dst) in enumerate(moves)]
    for load in loads:
        load.start()
    loads[0].wait()
    loads[1].wait()

    group_row = group_ref[...]
    rows8 = max(8, groups)
    onehot = (iota((rows8, tok), 0) == group_row).astype(F32)
    strict = (iota((tok, tok), 0) < iota((tok, tok), 1)).astype(F32)
    rank = jnp.dot(onehot.astype(BF16), strict.astype(BF16), preferred_element_type=F32)
    slot_row = jnp.sum(
        onehot * (iota((rows8, tok), 0).astype(F32) * cap + rank), axis=0, keepdims=True
    )
    picker = (iota((tok, tok), 0).astype(F32) == slot_row).astype(BF16)
    x = x_ref[...]
    xs[...] = jnp.dot(picker, x, preferred_element_type=F32).astype(BF16)

    def send(src, dst, sem, rsem, where):
        copy = pltpu.make_async_remote_copy(
            src_ref=src,
            dst_ref=dst,
            send_sem=send_sem.at[sem],
            recv_sem=rsem,
            device_id=where,
            device_id_type=MESH,
        )
        copy.start()

    def group_rows(e):
        return pl.ds(pl.multiple_of((e // per_group) * cap, cap), cap)

    def rows_of(first, count):
        return pl.ds(pl.multiple_of(first * cap, cap), count * cap)

    xr[pl.ds(0, cap), :] = xs[group_rows(me_e), :]

    def dispatch(c):
        for j in range(0 if c > 0 else 1, each):
            o, to = route(SEND, c, j)
            send(xs.at[group_rows(to)], xr.at[rows_of(o, 1)], 0, x_recv.at[o - 1], {"ep": to})

    def later():
        for c in range(AT_ONCE + 1, CHUNKS):
            dispatch(c)

    def enter():
        pl.semaphore_wait(barrier, n_ep - 1 + n_tp - 1)
        for c in range(AT_ONCE + 1):
            dispatch(c)
        if AT_ONCE + 1 < CHUNKS:
            pl.when(me_t % 2 == 0)(later)

    loads[2].wait()
    ngain = ngain_ref[...]
    squares = {}
    mate = {"tp": partner(me_t, 1, n_tp)}
    mine = pl.ds(pl.multiple_of(side * half, half), half)
    theirs = pl.ds(pl.multiple_of((1 - side) * half, half), half)
    body, tail = pl.ds(0, 2 * half), pl.ds(2 * half, LANES)

    def span(c):
        return rows_of(route(TAKE, c, 0)[0], each)

    def arrive(ref, sem):
        pltpu.make_async_copy(ref, ref, sem).wait()

    def stage_a(c):
        at = span(c)
        for j in range(0 if c > 0 else 1, each):
            o, _ = route(TAKE, c, j)
            arrive(xr.at[rows_of(o, 1)], x_recv.at[o - 1])
        vals = xr[at, :].astype(F32)
        squares[c] = jnp.sum(vals * vals, axis=1, keepdims=True)
        rows_in = (vals * ngain).astype(BF16)
        ps[at, pl.ds(0, half)] = jnp.dot(rows_in, wg[:, theirs], preferred_element_type=F32).astype(BF16)
        ps[at, pl.ds(half, half)] = jnp.dot(rows_in, wu[:, theirs], preferred_element_type=F32).astype(BF16)
        ps[at, tail] = pack(squares[c])
        if c > 0:
            send(ps.at[at], pr.at[at], 1, p_recv.at[c], mate)
        own[at, pl.ds(0, half)] = jnp.dot(rows_in, wg[:, mine], preferred_element_type=F32)
        own[at, pl.ds(half, half)] = jnp.dot(rows_in, wu[:, mine], preferred_element_type=F32)

    def stage_b(c):
        at = span(c)
        arrive(pr.at[at], p_recv.at[c])
        total = own[at, :] + pr[at, body].astype(F32)
        own[at, :] = total
        cs[at, body] = total.astype(BF16)
        squares[c] = squares[c] + unpack(pr[at, tail])
        cs[at, tail] = pack(squares[c])
        for i, s in enumerate(far):
            send(cs.at[at], cr.at[i, at], 2, c_recv.at[c, i], {"tp": partner(me_t, s, n_tp)})

    def stage_s(c):
        at = span(c)
        total, square = own[at, :], squares[c]
        for i in range(len(far)):
            arrive(cr.at[i, at], c_recv.at[c, i])
            total = total + cr[i, at, body].astype(F32)
            square = square + unpack(cr[i, at, tail])
        total = total * lax.rsqrt(square / full_width + EPS)
        g, u = total[:, :half], total[:, half:]
        hs[at, :] = (g / (1.0 + jnp.exp(-g)) * u).astype(BF16)
        send(hs.at[at], hr.at[at], 3, h_recv.at[c], mate)

    def stage_c(c):
        at = span(c)
        if c == 0:
            loads[8].wait()
        acc = jnp.dot(hs[at, :], wd[mine, :], preferred_element_type=F32)
        arrive(hr.at[at], h_recv.at[c])
        acc = acc + jnp.dot(hr[at, :], wd[theirs, :], preferred_element_type=F32)
        ob[at, :] = acc.astype(BF16)
        for j in range(0 if c > 0 else 1, each):
            o, to = route(TAKE, c, j)
            send(ob.at[rows_of(o, 1)], ret.at[rows_of(o, 1)], 4, o_recv.at[o - 1], {"ep": to})

    if each == 1:
        pl.when(quarter > 0)(enter)
    else:
        enter()
    loads[3].wait()
    loads[4].wait()
    stage_a(0)
    if each == 1:
        pl.when(quarter == 0)(enter)
    send(ps.at[span(0)], pr.at[span(0)], 1, p_recv.at[0], mate)
    for load in loads[5:8]:
        load.wait()
    scores = jnp.exp(score_ref[...])
    weights = prob_ref[...] * scores / jnp.sum(scores, axis=0, keepdims=True)
    slot_col = to_col(slot_row, tok).astype(jnp.int32)
    ids = group_row * per_group + member_ref[...]
    expert_cols = []
    for k in range(n_ep):
        named = jnp.where(ids == partner(me_e, k, n_ep), weights, 0.0)
        expert_cols.append(to_col(jnp.sum(named, axis=0, keepdims=True), tok))

    stages = {"a": stage_a, "b": stage_b, "s": stage_s, "c": stage_c}
    for stage, c in PLAN:
        stages[stage](c)
        if (stage, c) == ("a", 1) and AT_ONCE + 1 < CHUNKS:
            pl.when(me_t % 2 == 1)(later)

    summed = x.astype(F32)
    for k in [*range(each), *(q * each + j for q in BACK for j in range(each))]:
        e = partner(me_e, k, n_ep)
        block = pl.ds(k * cap, cap)
        if k > 0:
            arrive(ret.at[block], o_recv.at[k - 1])
            rows = ret[block, :]
        else:
            rows = ob[block, :]
        pick = (iota((tok, cap), 1) + (e // per_group) * cap == slot_col).astype(F32).astype(BF16)
        summed = summed + expert_cols[k] * jnp.dot(pick, rows, preferred_element_type=F32)

    square = jnp.sum(summed * summed, axis=1, keepdims=True)
    width = fs.shape[1]
    row = to_row(square, width)
    fs[...] = jnp.broadcast_to(row, (8, width))
    for s in range(1, n_tp):
        send(fs, fr.at[s - 1], 5, f_recv, {"tp": partner(me_t, s, n_tp)})

    arrive(fr, f_recv)
    for s in range(1, n_tp):
        row = row + fr[s - 1][0:1, :]
    out_ref[...] = summed * lax.rsqrt(to_col(row, tok) / full_width + EPS)

    others = pl.ds(cap, (n_ep - 1) * cap)
    for i, ref in enumerate((xr.at[others], pr, cr, hr, ret.at[others], fr)):
        arrive(ref, send_sem.at[i])


def solution(mesh):
    n_ep, n_tp = mesh.shape["ep"], mesh.shape["tp"]
    groups = max(2, n_ep // 8)
    n_far = n_tp // 2 - 1

    def local(tokens, group_choice, member_choice, group_prob, member_score, norm_gain, w_gate, w_up, w_down, final_gain):
        tok, dim = tokens.shape
        ff, top = w_gate.shape[2], member_choice.shape[1]
        cap = tok // groups
        all_rows = n_ep * cap
        out_width = -(-tok // 128) * 128
        vmem = pl.BlockSpec(memory_space=pltpu.VMEM)
        hbm = pl.BlockSpec(memory_space=pltpu.HBM)
        dma = pltpu.SemaphoreType.DMA
        normal = pl.pallas_call(
            functools.partial(kernel, (n_ep, n_tp, groups)),
            out_shape=pltpu.VMEM((tok, dim), F32),
            in_specs=[hbm] * 9,
            out_specs=vmem,
            scratch_shapes=[
                pltpu.VMEM((tok, dim), BF16),
                pltpu.VMEM((1, tok), jnp.int32),
                pltpu.VMEM((top, tok), jnp.int32),
                pltpu.VMEM((1, tok), F32),
                pltpu.VMEM((top, tok), F32),
                pltpu.VMEM((1, dim), F32),
                pltpu.VMEM((dim, ff), BF16),
                pltpu.VMEM((dim, ff), BF16),
                pltpu.VMEM((ff, dim), BF16),
                pltpu.VMEM((tok, dim), BF16),
                pltpu.VMEM((all_rows, dim), BF16),
                pltpu.VMEM((all_rows, ff + LANES), BF16),
                pltpu.VMEM((all_rows, ff + LANES), BF16),
                pltpu.VMEM((all_rows, ff), F32),
                pltpu.VMEM((all_rows, ff + LANES), BF16),
                pltpu.VMEM((n_far, all_rows, ff + LANES), BF16),
                pltpu.VMEM((all_rows, ff // 2), BF16),
                pltpu.VMEM((all_rows, ff // 2), BF16),
                pltpu.VMEM((all_rows, dim), BF16),
                pltpu.VMEM((all_rows, dim), BF16),
                pltpu.VMEM((8, out_width), F32),
                pltpu.VMEM((n_tp - 1, 8, out_width), F32),
                dma((9,)),
                dma((6,)),
                dma((n_ep - 1,)),
                dma((CHUNKS,)),
                dma((CHUNKS, n_far)),
                dma((CHUNKS,)),
                dma((n_ep - 1,)),
                dma,
            ],
            compiler_params=pltpu.CompilerParams(collective_id=0, has_side_effects=True, vmem_limit_bytes=VMEM_LIMIT),
        )(
            tokens,
            group_choice.reshape(1, tok),
            member_choice.T,
            group_prob.reshape(1, tok),
            member_score.T,
            norm_gain.reshape(1, dim),
            w_gate,
            w_up,
            w_down,
        )
        return (normal * final_gain[None, :]).astype(BF16)

    return jax.shard_map(
        local,
        mesh=mesh,
        in_specs=(
            P(("grp", "ep"), "tp"),
            P(("grp", "ep")),
            P(("grp", "ep"), None),
            P(("grp", "ep")),
            P(("grp", "ep"), None),
            P("tp"),
            P("ep", "tp", None),
            P("ep", "tp", None),
            P("ep", None, "tp"),
            P("tp"),
        ),
        out_specs=P(("grp", "ep"), "tp"),
        check_vma=False,
    )
```

time: 30.3 us -> 27 us (0.89)
  Pallas kernels: 29.4 us -> 26.1 us
    pallas_call x1, Pallas kernels: 29.4 us -> 26.1 us  [local(): pl.pallas_call(functools.partial(kernel, (n_ep, n_tp, groups)), out_shape...]
where the time goes in v1:
time: 27 us; the launch traced here: 26.8 us
  Pallas kernels  26.1 us (97%)
  other arithmetic  0.67 us (2%)
    pallas_call x1, Pallas kernels, local(): pl.pallas_call(functools.partial(kernel, (n_ep, n_tp, groups)), out_shape...  26.1 us
    convert_element_type x1, other arithmetic, local(): return (normal * final_gain[None, :]).astype(BF16)  0.67 us

profile of v1, /device:TPU:0, one launch (start us, length us, event | category | flops | bytes accessed | tf_op | source)
XLA Modules:
  0.0 26.8 jit_solution(13298041663084643851)
XLA Ops:
  0.0 0.0 copy-start
  0.0 26.1 %shard_map.100 = f32[64,1024]{1,0:T(8,128)S(1)} custom-call(bf16[64,1024]{1,0:T(8,128)(2,1)} %x_hbm.1, s32[1,64]{1,0:T(1,128)} %bitcast.8, s32[2,64]{1,0:T(2,128)} %bitcast.6, f32[1,64]{1,0:T(1,128)} %bitcast.9, f32[2,64]{1,0:T(2,128)} %bitcast.7, f32[1,1024]{1,0:T(1,128)} %bitcast.5, bf16[1,1024,1024]{2,1,0:T(8,128)(2,1)} %wg_hbm.1, ...), custom_call_target="tpu_custom_call" | custom-call | tf_op jit(solution)/shard_map/pallas_call | solution.py:345
  26.1 0.0 copy-done
  26.1 0.7 %multiply_convert_fusion = bf16[64,1024]{1,0:T(8,128)(2,1)} fusion(f32[64,1024]{1,0:T(8,128)S(1)} %shard_map.100, f32[1024]{0:T(1024)S(1)} %copy-done), kind=kLoop, calls=%fused_computation | loop fusion | flops 131072 | bytes 397312 | tf_op jit(solution)/shard_map/convert_element_type | solution.py:394
Async XLA Ops:
  0.0 26.1 %copy-start = (f32[1024]{0:T(1024)S(1)}, f32[1024]{0:T(1024)}, u32[]{:S(2)}) copy-start(f32[1024]{0:T(1024)} %param.19) | copy-start | bytes 12292

commit v2 on v1

--- a/solution.py
+++ b/solution.py
@@ -15,12 +15,21 @@
 TAKE = ((1, 2, 3), (1, 3, 2), (3, 2, 1), (1, 3, 2))
 BACK = (2, 3, 1)
 AT_ONCE = 2
+EVEN_PLAN = (
+    ("b", 0), ("f", 0), ("a", 1), ("b", 1), ("a", 2), ("b", 2), ("s", 0), ("a", 3), ("c", 0), ("b", 3),
+)
+ODD_PLAN = (
+    ("b", 0), ("f", 0), ("a", 1), ("a", 2), ("b", 1), ("a", 3), ("s", 0), ("b", 2), ("b", 3), ("c", 0),
+)
 PLAN = (
-    ("b", 0), ("a", 1), ("b", 1), ("a", 2), ("s", 0), ("b", 2), ("a", 3),
-    ("c", 0), ("b", 3), ("s", 1), ("c", 1), ("s", 2), ("c", 2), ("s", 3), ("c", 3),
+    ("s", 1), ("c", 1), ("s", 2), ("c", 2), ("s", 3), ("c", 3),
 )
 LANES = 128
 CHUNKS = 4
+PIECES = 2
+FIRST = 2
+RELAY_SEND = (2, 1)
+RELAY_TAKE = ((2, 1, 3), (1, 2, 3), (2, 1, 3), (2, 3, 1))
 VMEM_LIMIT = 56 * 2**20
 
 
@@ -102,6 +111,8 @@
     hr,
     ob,
     ret,
+    total_ref,
+    split,
     fs,
     fr,
     w_sem,
@@ -124,6 +135,9 @@
     side = parity(me_t, n_tp)
     far = [s for s in range(1, n_tp) if parity(s, n_tp) == 0]
     each = n_ep // CHUNKS
+    relay = each == 1 and per_group == 2
+    take = RELAY_TAKE if relay else TAKE
+    met = [s for s in range(1, n_ep) if not relay or s < 3]
     quarter = me_e // each
 
     def by_quarter(values):
@@ -138,7 +152,7 @@
         return by_quarter(step) * each + j, to
 
     barrier = pltpu.get_barrier_semaphore()
-    for s in range(1, n_ep):
+    for s in met:
         pl.semaphore_signal(barrier, inc=1, device_id={"ep": partner(me_e, s, n_ep)}, device_id_type=MESH)
     for s in range(1, n_tp):
         pl.semaphore_signal(barrier, inc=1, device_id={"tp": partner(me_t, s, n_tp)}, device_id_type=MESH)
@@ -158,8 +172,6 @@
     for load in loads:
         load.start()
     loads[0].wait()
-    loads[1].wait()
-
     group_row = group_ref[...]
     rows8 = max(8, groups)
     onehot = (iota((rows8, tok), 0) == group_row).astype(F32)
@@ -169,8 +181,8 @@
         onehot * (iota((rows8, tok), 0).astype(F32) * cap + rank), axis=0, keepdims=True
     )
     picker = (iota((tok, tok), 0).astype(F32) == slot_row).astype(BF16)
-    x = x_ref[...]
-    xs[...] = jnp.dot(picker, x, preferred_element_type=F32).astype(BF16)
+    loads[1].wait()
+    xs[...] = jnp.dot(picker, x_ref[...], preferred_element_type=F32).astype(BF16)
 
     def send(src, dst, sem, rsem, where):
         copy = pltpu.make_async_remote_copy(
@@ -183,6 +195,9 @@
         )
         copy.start()
 
+    def arrive(ref, sem):
+        pltpu.make_async_copy(ref, ref, sem).wait()
+
     def group_rows(e):
         return pl.ds(pl.multiple_of((e // per_group) * cap, cap), cap)
 
@@ -194,14 +209,29 @@
     def dispatch(c):
         for j in range(0 if c > 0 else 1, each):
             o, to = route(SEND, c, j)
-            send(xs.at[group_rows(to)], xr.at[rows_of(o, 1)], 0, x_recv.at[o - 1], {"ep": to})
+            send(xs.at[group_rows(to)], xr.at[rows_of(o, 1)], 0, x_recv.at[o - 1, 0], {"ep": to})
+
+    def piece(ref, block, p):
+        rows = cap // PIECES
+        return ref.at[pl.ds(pl.multiple_of(block * cap + p * rows, rows), rows)]
+
+    def stage_f(c):
+        for p in range(PIECES):
+            arrive(piece(xr, 2, p), x_recv.at[1, p])
+            send(piece(xr, 2, p), piece(xr, 3, p), 0, x_recv.at[2, p], {"ep": partner(me_e, 1, n_ep)})
 
     def later():
         for c in range(AT_ONCE + 1, CHUNKS):
             dispatch(c)
 
     def enter():
-        pl.semaphore_wait(barrier, n_ep - 1 + n_tp - 1)
+        pl.semaphore_wait(barrier, len(met) + n_tp - 1)
+        if relay:
+            for o in RELAY_SEND:
+                to = partner(me_e, o, n_ep)
+                for p in range(PIECES):
+                    send(piece(xs, to // per_group, p), piece(xr, o, p), 0, x_recv.at[o - 1, p], {"ep": to})
+            return
         for c in range(AT_ONCE + 1):
             dispatch(c)
         if AT_ONCE + 1 < CHUNKS:
@@ -209,29 +239,32 @@
 
     loads[2].wait()
     ngain = ngain_ref[...]
-    squares = {}
     mate = {"tp": partner(me_t, 1, n_tp)}
     mine = pl.ds(pl.multiple_of(side * half, half), half)
     theirs = pl.ds(pl.multiple_of((1 - side) * half, half), half)
     body, tail = pl.ds(0, 2 * half), pl.ds(2 * half, LANES)
 
     def span(c):
-        return rows_of(route(TAKE, c, 0)[0], each)
-
-    def arrive(ref, sem):
-        pltpu.make_async_copy(ref, ref, sem).wait()
+        return rows_of(route(take, c, 0)[0], each)
 
     def stage_a(c):
         at = span(c)
-        for j in range(0 if c > 0 else 1, each):
-            o, _ = route(TAKE, c, j)
-            arrive(xr.at[rows_of(o, 1)], x_recv.at[o - 1])
+        if relay and c > 0:
+            o, _ = route(take, c, 0)
+
+            def landed():
+                for p in range(PIECES):
+                    arrive(piece(xr, o, p), x_recv.at[o - 1, p])
+
+            pl.when(o != 2)(landed)
+        for j in range(each if relay else 0 if c > 0 else 1, each):
+            o, _ = route(take, c, j)
+            arrive(xr.at[rows_of(o, 1)], x_recv.at[o - 1, 0])
         vals = xr[at, :].astype(F32)
-        squares[c] = jnp.sum(vals * vals, axis=1, keepdims=True)
         rows_in = (vals * ngain).astype(BF16)
         ps[at, pl.ds(0, half)] = jnp.dot(rows_in, wg[:, theirs], preferred_element_type=F32).astype(BF16)
         ps[at, pl.ds(half, half)] = jnp.dot(rows_in, wu[:, theirs], preferred_element_type=F32).astype(BF16)
-        ps[at, tail] = pack(squares[c])
+        ps[at, tail] = pack(jnp.sum(vals * vals, axis=1, keepdims=True))
         if c > 0:
             send(ps.at[at], pr.at[at], 1, p_recv.at[c], mate)
         own[at, pl.ds(0, half)] = jnp.dot(rows_in, wg[:, mine], preferred_element_type=F32)
@@ -243,14 +276,13 @@
         total = own[at, :] + pr[at, body].astype(F32)
         own[at, :] = total
         cs[at, body] = total.astype(BF16)
-        squares[c] = squares[c] + unpack(pr[at, tail])
-        cs[at, tail] = pack(squares[c])
+        cs[at, tail] = pack(unpack(ps[at, tail]) + unpack(pr[at, tail]))
         for i, s in enumerate(far):
             send(cs.at[at], cr.at[i, at], 2, c_recv.at[c, i], {"tp": partner(me_t, s, n_tp)})
 
     def stage_s(c):
         at = span(c)
-        total, square = own[at, :], squares[c]
+        total, square = own[at, :], unpack(cs[at, tail])
         for i in range(len(far)):
             arrive(cr.at[i, at], c_recv.at[c, i])
             total = total + cr[i, at, body].astype(F32)
@@ -269,48 +301,55 @@
         acc = acc + jnp.dot(hr[at, :], wd[theirs, :], preferred_element_type=F32)
         ob[at, :] = acc.astype(BF16)
         for j in range(0 if c > 0 else 1, each):
-            o, to = route(TAKE, c, j)
+            o, to = route(take, c, j)
             send(ob.at[rows_of(o, 1)], ret.at[rows_of(o, 1)], 4, o_recv.at[o - 1], {"ep": to})
 
     if each == 1:
-        pl.when(quarter > 0)(enter)
+        pl.when(me_e * n_tp + me_t >= FIRST)(enter)
     else:
         enter()
     loads[3].wait()
     loads[4].wait()
     stage_a(0)
     if each == 1:
-        pl.when(quarter == 0)(enter)
+        pl.when(me_e * n_tp + me_t < FIRST)(enter)
     send(ps.at[span(0)], pr.at[span(0)], 1, p_recv.at[0], mate)
     for load in loads[5:8]:
         load.wait()
     scores = jnp.exp(score_ref[...])
     weights = prob_ref[...] * scores / jnp.sum(scores, axis=0, keepdims=True)
-    slot_col = to_col(slot_row, tok).astype(jnp.int32)
+    slots = slot_row.astype(jnp.int32)
     ids = group_row * per_group + member_ref[...]
     expert_cols = []
     for k in range(n_ep):
-        named = jnp.where(ids == partner(me_e, k, n_ep), weights, 0.0)
-        expert_cols.append(to_col(jnp.sum(named, axis=0, keepdims=True), tok))
-
-    stages = {"a": stage_a, "b": stage_b, "s": stage_s, "c": stage_c}
-    for stage, c in PLAN:
-        stages[stage](c)
-        if (stage, c) == ("a", 1) and AT_ONCE + 1 < CHUNKS:
-            pl.when(me_t % 2 == 1)(later)
-
-    summed = x.astype(F32)
+        e = partner(me_e, k, n_ep)
+        named = jnp.sum(jnp.where(ids == e, weights, 0.0), axis=0, keepdims=True)
+        here = iota((cap, tok), 0) + (e // per_group) * cap == slots
+        expert_cols.append(jnp.sum(jnp.where(here, named, 0.0), axis=1, keepdims=True))
+    slot_col = to_col(slot_row, tok).astype(jnp.int32)
+    total_ref[...] = xs[...].astype(F32)
+
+    stages = {"f": stage_f, "a": stage_a, "b": stage_b, "s": stage_s, "c": stage_c}
+    def run(plan):
+        for stage, c in plan:
+            if relay or stage != "f":
+                stages[stage](c)
+            if (stage, c) == ("a", 1) and not relay and AT_ONCE + 1 < CHUNKS:
+                pl.when(me_t % 2 == 1)(later)
+
+    pl.when(me_t % 2 == 0)(functools.partial(run, EVEN_PLAN))
+    pl.when(me_t % 2 == 1)(functools.partial(run, ODD_PLAN))
+    run(PLAN)
+
     for k in [*range(each), *(q * each + j for q in BACK for j in range(each))]:
-        e = partner(me_e, k, n_ep)
         block = pl.ds(k * cap, cap)
         if k > 0:
             arrive(ret.at[block], o_recv.at[k - 1])
-            rows = ret[block, :]
-        else:
-            rows = ob[block, :]
-        pick = (iota((tok, cap), 1) + (e // per_group) * cap == slot_col).astype(F32).astype(BF16)
-        summed = summed + expert_cols[k] * jnp.dot(pick, rows, preferred_element_type=F32)
-
+        rows = (ret if k > 0 else ob)[block, :].astype(F32)
+        at = group_rows(partner(me_e, k, n_ep))
+        total_ref[at, :] = total_ref[at, :] + expert_cols[k] * rows
+
+    summed = total_ref[...]
     square = jnp.sum(summed * summed, axis=1, keepdims=True)
     width = fs.shape[1]
     row = to_row(square, width)
@@ -318,10 +357,21 @@
     for s in range(1, n_tp):
         send(fs, fr.at[s - 1], 5, f_recv, {"tp": partner(me_t, s, n_tp)})
 
+    high = summed.astype(BF16)
+    rest = summed - high.astype(F32)
+    middle = rest.astype(BF16)
+    split[pl.ds(0, tok), :] = high
+    split[pl.ds(tok, tok), :] = middle
+    split[pl.ds(2 * tok, tok), :] = (rest - middle.astype(F32)).astype(BF16)
+    lanes = iota((tok, 3 * tok), 1)
+    back = jnp.where(lanes < tok, lanes, jnp.where(lanes < 2 * tok, lanes - tok, lanes - 2 * tok)) == slot_col
+    out_ref[...] = jnp.dot(back.astype(F32).astype(BF16), split[...], preferred_element_type=F32)
+
     arrive(fr, f_recv)
     for s in range(1, n_tp):
         row = row + fr[s - 1][0:1, :]
-    out_ref[...] = summed * lax.rsqrt(to_col(row, tok) / full_width + EPS)
+    square = jnp.sum(jnp.where(iota((tok, width), 1) == slot_col, row, 0.0), axis=1, keepdims=True)
+    out_ref[...] = out_ref[...] * lax.rsqrt(square / full_width + EPS)
 
     others = pl.ds(cap, (n_ep - 1) * cap)
     for i, ref in enumerate((xr.at[others], pr, cr, hr, ret.at[others], fr)):
@@ -368,11 +418,13 @@
                 pltpu.VMEM((all_rows, ff // 2), BF16),
                 pltpu.VMEM((all_rows, dim), BF16),
                 pltpu.VMEM((all_rows, dim), BF16),
+                pltpu.VMEM((tok, dim), F32),
+                pltpu.VMEM((3 * tok, dim), BF16),
                 pltpu.VMEM((8, out_width), F32),
                 pltpu.VMEM((n_tp - 1, 8, out_width), F32),
                 dma((9,)),
                 dma((6,)),
-                dma((n_ep - 1,)),
+                dma((n_ep - 1, PIECES)),
                 dma((CHUNKS,)),
                 dma((CHUNKS, n_far)),
                 dma((CHUNKS,)),

time: 27 us -> 26.7 us (0.989)
  Pallas kernels: 26.1 us -> 25.8 us
where the time goes in v2:
time: 26.7 us; the launch traced here: 26.5 us
  Pallas kernels  25.8 us (97%)
  other arithmetic  0.67 us (3%)
    pallas_call x1, Pallas kernels, local(): pl.pallas_call(functools.partial(kernel, (n_ep, n_tp, groups)), out_shape...  25.8 us
    convert_element_type x1, other arithmetic, local(): return (normal * final_gain[None, :]).astype(BF16)  0.67 us

profile of v2, /device:TPU:0, one launch (start us, length us, event | category | flops | bytes accessed | tf_op | source)
XLA Modules:
  0.0 26.5 jit_solution(6473300106068534038)
XLA Ops:
  0.0 0.0 copy-start
  0.0 25.8 %shard_map.100 = f32[64,1024]{1,0:T(8,128)S(1)} custom-call(bf16[64,1024]{1,0:T(8,128)(2,1)} %x_hbm.1, s32[1,64]{1,0:T(1,128)} %bitcast.8, s32[2,64]{1,0:T(2,128)} %bitcast.6, f32[1,64]{1,0:T(1,128)} %bitcast.9, f32[2,64]{1,0:T(2,128)} %bitcast.7, f32[1,1024]{1,0:T(1,128)} %bitcast.5, bf16[1,1024,1024]{2,1,0:T(8,128)(2,1)} %wg_hbm.1, ...), custom_call_target="tpu_custom_call" | custom-call | tf_op jit(solution)/shard_map/pallas_call | solution.py:395
  25.9 0.0 copy-done
  25.9 0.7 %multiply_convert_fusion = bf16[64,1024]{1,0:T(8,128)(2,1)} fusion(f32[64,1024]{1,0:T(8,128)S(1)} %shard_map.100, f32[1024]{0:T(1024)S(1)} %copy-done), kind=kLoop, calls=%fused_computation | loop fusion | flops 131072 | bytes 397312 | tf_op jit(solution)/shard_map/convert_element_type | solution.py:446
Async XLA Ops:
  0.0 25.9 %copy-start = (f32[1024]{0:T(1024)S(1)}, f32[1024]{0:T(1024)}, u32[]{:S(2)}) copy-start(f32[1024]{0:T(1024)} %param.19) | copy-start | bytes 12292

commit v3 on v2

--- a/solution.py
+++ b/solution.py
@@ -16,18 +16,22 @@
 BACK = (2, 3, 1)
 AT_ONCE = 2
 EVEN_PLAN = (
-    ("b", 0), ("f", 0), ("a", 1), ("b", 1), ("a", 2), ("b", 2), ("s", 0), ("a", 3), ("c", 0), ("b", 3),
+    ("b", 0), ("w", 0), ("f", 0), ("a", 1), ("w", 1), ("b", 1), ("a", 2), ("w", 2), ("b", 2), ("s", 0), ("a", 3), ("w", 3), ("b", 3),
 )
 ODD_PLAN = (
-    ("b", 0), ("f", 0), ("a", 1), ("a", 2), ("b", 1), ("a", 3), ("s", 0), ("b", 2), ("b", 3), ("c", 0),
+    ("b", 0), ("f", 0), ("a", 1), ("a", 2), ("b", 1), ("a", 3), ("s", 0), ("b", 2), ("b", 3),
 )
 PLAN = (
-    ("s", 1), ("c", 1), ("s", 2), ("c", 2), ("s", 3), ("c", 3),
+    ("s", 1), ("c", 1), ("s", 2), ("c", 2), ("s", 3), ("c", 3), ("c", 0),
 )
 LANES = 128
 CHUNKS = 4
 PIECES = 2
 FIRST = 2
+W_PIECES = 8
+W_CUTS = ((0, 2), (2, 4), (4, 6), (6, 8))
+C_FIRST = 1
+EARLY = 4
 RELAY_SEND = (2, 1)
 RELAY_TAKE = ((2, 1, 3), (1, 2, 3), (2, 1, 3), (2, 3, 1))
 VMEM_LIMIT = 56 * 2**20
@@ -99,7 +103,7 @@
     ngain_ref,
     wg,
     wu,
-    wd,
+    wds,
     xs,
     xr,
     ps,
@@ -108,7 +112,6 @@
     cs,
     cr,
     hs,
-    hr,
     ob,
     ret,
     total_ref,
@@ -120,21 +123,25 @@
     x_recv,
     p_recv,
     c_recv,
-    h_recv,
     o_recv,
     f_recv,
+    wd_recv,
 ):
     n_ep, n_tp, groups = cfg
     per_group = n_ep // groups
     tok, dim = x_ref.shape
     cap = tok // groups
-    half = wg.shape[1] // 2
+    ff = wg.shape[1]
     full_width = dim * n_tp
     me_e = lax.axis_index("ep")
     me_t = lax.axis_index("tp")
     side = parity(me_t, n_tp)
     far = [s for s in range(1, n_tp) if parity(s, n_tp) == 0]
     each = n_ep // CHUNKS
+    count = each * cap // 2
+    units = max(1, each // 2)
+    unit = count // units
+    odd = me_t % 2
     relay = each == 1 and per_group == 2
     take = RELAY_TAKE if relay else TAKE
     met = [s for s in range(1, n_ep) if not relay or s < 3]
@@ -166,7 +173,7 @@
         (member_hbm, member_ref),
         (prob_hbm, prob_ref),
         (score_hbm, score_ref),
-        (wd_hbm.at[0], wd),
+        (wd_hbm.at[0], wds.at[odd]),
     )
     loads = [pltpu.make_async_copy(src, dst, w_sem.at[i]) for i, (src, dst) in enumerate(moves)]
     for load in loads:
@@ -224,7 +231,7 @@
         for c in range(AT_ONCE + 1, CHUNKS):
             dispatch(c)
 
-    def enter():
+    def greet():
         pl.semaphore_wait(barrier, len(met) + n_tp - 1)
         if relay:
             for o in RELAY_SEND:
@@ -237,12 +244,22 @@
         if AT_ONCE + 1 < CHUNKS:
             pl.when(me_t % 2 == 0)(later)
 
+    def enter():
+        greet()
+        if EARLY:
+            pl.when(odd == 1)(push)
+
+    def push():
+        for c in range(EARLY):
+            stage_w(c)
+
     loads[2].wait()
     ngain = ngain_ref[...]
     mate = {"tp": partner(me_t, 1, n_tp)}
-    mine = pl.ds(pl.multiple_of(side * half, half), half)
-    theirs = pl.ds(pl.multiple_of((1 - side) * half, half), half)
-    body, tail = pl.ds(0, 2 * half), pl.ds(2 * half, LANES)
+    body, tail = pl.ds(0, 2 * ff), pl.ds(2 * ff, LANES)
+
+    def mine(c):
+        return pl.ds(c * count, count)
 
     def span(c):
         return rows_of(route(take, c, 0)[0], each)
@@ -262,47 +279,77 @@
             arrive(xr.at[rows_of(o, 1)], x_recv.at[o - 1, 0])
         vals = xr[at, :].astype(F32)
         rows_in = (vals * ngain).astype(BF16)
-        ps[at, pl.ds(0, half)] = jnp.dot(rows_in, wg[:, theirs], preferred_element_type=F32).astype(BF16)
-        ps[at, pl.ds(half, half)] = jnp.dot(rows_in, wu[:, theirs], preferred_element_type=F32).astype(BF16)
-        ps[at, tail] = pack(jnp.sum(vals * vals, axis=1, keepdims=True))
+        square = jnp.sum(vals * vals, axis=1, keepdims=True)
+        gate = jnp.dot(rows_in, wg[...], preferred_element_type=F32)
+        up = jnp.dot(rows_in, wu[...], preferred_element_type=F32)
+
+        def part(of, whose):
+            return jnp.where(whose == 0, of[:count], of[count:])
+
+        ps[mine(c), pl.ds(0, ff)] = part(gate, 1 - side).astype(BF16)
+        ps[mine(c), pl.ds(ff, ff)] = part(up, 1 - side).astype(BF16)
+        ps[mine(c), tail] = pack(part(square, 1 - side))
         if c > 0:
-            send(ps.at[at], pr.at[at], 1, p_recv.at[c], mate)
-        own[at, pl.ds(0, half)] = jnp.dot(rows_in, wg[:, mine], preferred_element_type=F32)
-        own[at, pl.ds(half, half)] = jnp.dot(rows_in, wu[:, mine], preferred_element_type=F32)
+            send(ps.at[mine(c)], pr.at[mine(c)], 1, p_recv.at[c], mate)
+        own[mine(c), pl.ds(0, ff)] = part(gate, side)
+        own[mine(c), pl.ds(ff, ff)] = part(up, side)
+        own[mine(c), tail] = jnp.broadcast_to(part(square, side), (count, LANES))
 
     def stage_b(c):
-        at = span(c)
+        at = mine(c)
         arrive(pr.at[at], p_recv.at[c])
-        total = own[at, :] + pr[at, body].astype(F32)
-        own[at, :] = total
+        total = own[at, body] + pr[at, body].astype(F32)
+        own[at, body] = total
         cs[at, body] = total.astype(BF16)
-        cs[at, tail] = pack(unpack(ps[at, tail]) + unpack(pr[at, tail]))
+        square = own[at, tail] + unpack(pr[at, tail])
+        own[at, tail] = square
+        cs[at, tail] = pack(square[:, :1])
         for i, s in enumerate(far):
             send(cs.at[at], cr.at[i, at], 2, c_recv.at[c, i], {"tp": partner(me_t, s, n_tp)})
 
     def stage_s(c):
-        at = span(c)
-        total, square = own[at, :], unpack(cs[at, tail])
+        at = mine(c)
+        total, square = own[at, body], own[at, tail]
         for i in range(len(far)):
             arrive(cr.at[i, at], c_recv.at[c, i])
             total = total + cr[i, at, body].astype(F32)
             square = square + unpack(cr[i, at, tail])
-        total = total * lax.rsqrt(square / full_width + EPS)
-        g, u = total[:, :half], total[:, half:]
+        total = total * lax.rsqrt(square[:, :1] / full_width + EPS)
+        g, u = total[:, :ff], total[:, ff:]
         hs[at, :] = (g / (1.0 + jnp.exp(-g)) * u).astype(BF16)
-        send(hs.at[at], hr.at[at], 3, h_recv.at[c], mate)
+
+    def stage_w(c):
+        piece_rows = ff // W_PIECES
+        for p in range(*W_CUTS[c]):
+            rows = pl.ds(p * piece_rows, piece_rows)
+            send(wd_hbm.at[0, rows], wds.at[odd, rows], 3, wd_recv, mate)
 
     def stage_c(c):
-        at = span(c)
-        if c == 0:
+        if c == C_FIRST:
             loads[8].wait()
-        acc = jnp.dot(hs[at, :], wd[mine, :], preferred_element_type=F32)
-        arrive(hr.at[at], h_recv.at[c])
-        acc = acc + jnp.dot(hr[at, :], wd[theirs, :], preferred_element_type=F32)
-        ob[at, :] = acc.astype(BF16)
-        for j in range(0 if c > 0 else 1, each):
-            o, to = route(take, c, j)
-            send(ob.at[rows_of(o, 1)], ret.at[rows_of(o, 1)], 4, o_recv.at[o - 1], {"ep": to})
+            arrive(wds.at[1 - odd], wd_recv)
+        hidden = hs[mine(c), :]
+        for q in range(2):
+            ob[q, mine(c), :] = jnp.dot(hidden, wds[q], preferred_element_type=F32).astype(BF16)
+            for j in range(units):
+                low, high = route(take, c, j), route(take, c, j + units if each > 1 else 0)
+                o, to = (a + side * (b - a) for a, b in zip(low, high))
+                block = o * (cap // unit) + (side if each == 1 else 0)
+                src = ob.at[q, pl.ds(c * count + j * unit, unit)]
+                dst = ret.at[pl.ds(pl.multiple_of(block * unit, unit), unit)]
+
+                def stay():
+                    dst[...] = src[...]
+
+                def away():
+                    send(src, dst, 4, o_recv.at[block], {"ep": to, "tp": me_t - odd + q})
+
+                if c + j > 0:
+                    away()
+                else:
+                    home = (odd == q) & (to == me_e)
+                    pl.when(home)(stay)
+                    pl.when(jnp.logical_not(home))(away)
 
     if each == 1:
         pl.when(me_e * n_tp + me_t >= FIRST)(enter)
@@ -313,7 +360,7 @@
     stage_a(0)
     if each == 1:
         pl.when(me_e * n_tp + me_t < FIRST)(enter)
-    send(ps.at[span(0)], pr.at[span(0)], 1, p_recv.at[0], mate)
+    send(ps.at[mine(0)], pr.at[mine(0)], 1, p_recv.at[0], mate)
     for load in loads[5:8]:
         load.wait()
     scores = jnp.exp(score_ref[...])
@@ -329,7 +376,7 @@
     slot_col = to_col(slot_row, tok).astype(jnp.int32)
     total_ref[...] = xs[...].astype(F32)
 
-    stages = {"f": stage_f, "a": stage_a, "b": stage_b, "s": stage_s, "c": stage_c}
+    stages = {"w": stage_w, "f": stage_f, "a": stage_a, "b": stage_b, "s": stage_s, "c": stage_c}
     def run(plan):
         for stage, c in plan:
             if relay or stage != "f":
@@ -344,8 +391,15 @@
     for k in [*range(each), *(q * each + j for q in BACK for j in range(each))]:
         block = pl.ds(k * cap, cap)
         if k > 0:
-            arrive(ret.at[block], o_recv.at[k - 1])
-        rows = (ret if k > 0 else ob)[block, :].astype(F32)
+            for h in range(cap // unit):
+                b = k * (cap // unit) + h
+                arrive(ret.at[pl.ds(b * unit, unit)], o_recv.at[b])
+        elif each == 1:
+            b = 1 - side
+            arrive(ret.at[pl.ds(pl.multiple_of(b * unit, unit), unit)], o_recv.at[b])
+        else:
+            pl.when(side == 1)(lambda: arrive(ret.at[pl.ds(0, unit)], o_recv.at[0]))
+        rows = ret[block, :].astype(F32)
         at = group_rows(partner(me_e, k, n_ep))
         total_ref[at, :] = total_ref[at, :] + expert_cols[k] * rows
 
@@ -374,8 +428,11 @@
     out_ref[...] = out_ref[...] * lax.rsqrt(square / full_width + EPS)
 
     others = pl.ds(cap, (n_ep - 1) * cap)
-    for i, ref in enumerate((xr.at[others], pr, cr, hr, ret.at[others], fr)):
+    returns = pl.ds(unit, n_ep * cap - unit)
+    for i, ref in enumerate((xr.at[others], pr, cr, wds.at[0], ret.at[returns], fr)):
         arrive(ref, send_sem.at[i])
+    if each > 1:
+        pl.when(side == 1)(lambda: arrive(ret.at[pl.ds(0, unit)], send_sem.at[4]))
 
 
 def solution(mesh):
@@ -388,6 +445,7 @@
         ff, top = w_gate.shape[2], member_choice.shape[1]
         cap = tok // groups
         all_rows = n_ep * cap
+        unit = min(cap, all_rows // CHUNKS // 2)
         out_width = -(-tok // 128) * 128
         vmem = pl.BlockSpec(memory_space=pltpu.VMEM)
         hbm = pl.BlockSpec(memory_space=pltpu.HBM)
@@ -406,17 +464,16 @@
                 pltpu.VMEM((1, dim), F32),
                 pltpu.VMEM((dim, ff), BF16),
                 pltpu.VMEM((dim, ff), BF16),
-                pltpu.VMEM((ff, dim), BF16),
+                pltpu.VMEM((2, ff, dim), BF16),
                 pltpu.VMEM((tok, dim), BF16),
                 pltpu.VMEM((all_rows, dim), BF16),
-                pltpu.VMEM((all_rows, ff + LANES), BF16),
-                pltpu.VMEM((all_rows, ff + LANES), BF16),
-                pltpu.VMEM((all_rows, ff), F32),
-                pltpu.VMEM((all_rows, ff + LANES), BF16),
-                pltpu.VMEM((n_far, all_rows, ff + LANES), BF16),
-                pltpu.VMEM((all_rows, ff // 2), BF16),
-                pltpu.VMEM((all_rows, ff // 2), BF16),
-                pltpu.VMEM((all_rows, dim), BF16),
+                pltpu.VMEM((all_rows // 2, 2 * ff + LANES), BF16),
+                pltpu.VMEM((all_rows // 2, 2 * ff + LANES), BF16),
+                pltpu.VMEM((all_rows // 2, 2 * ff + LANES), F32),
+                pltpu.VMEM((all_rows // 2, 2 * ff + LANES), BF16),
+                pltpu.VMEM((n_far, all_rows // 2, 2 * ff + LANES), BF16),
+                pltpu.VMEM((all_rows // 2, ff), BF16),
+                pltpu.VMEM((2, all_rows // 2, dim), BF16),
                 pltpu.VMEM((all_rows, dim), BF16),
                 pltpu.VMEM((tok, dim), F32),
                 pltpu.VMEM((3 * tok, dim), BF16),
@@ -427,8 +484,8 @@
                 dma((n_ep - 1, PIECES)),
                 dma((CHUNKS,)),
                 dma((CHUNKS, n_far)),
-                dma((CHUNKS,)),
-                dma((n_ep - 1,)),
+                dma((all_rows // unit,)),
+                dma,
                 dma,
             ],
             compiler_params=pltpu.CompilerParams(collective_id=0, has_side_effects=True, vmem_limit_bytes=VMEM_LIMIT),

time: 26.7 us -> 25.4 us (0.951)
  Pallas kernels: 25.8 us -> 24.6 us
    pallas_call x1, Pallas kernels: 25.8 us -> 24.6 us  [local(): pl.pallas_call(functools.partial(kernel, (n_ep, n_tp, groups)), out_shape...]
where the time goes in v3:
time: 25.4 us; the launch traced here: 25.3 us
  Pallas kernels  24.6 us (97%)
  other arithmetic  0.67 us (3%)
    pallas_call x1, Pallas kernels, local(): pl.pallas_call(functools.partial(kernel, (n_ep, n_tp, groups)), out_shape...  24.6 us
    convert_element_type x1, other arithmetic, local(): return (normal * final_gain[None, :]).astype(BF16)  0.67 us

profile of v3, /device:TPU:0, one launch (start us, length us, event | category | flops | bytes accessed | tf_op | source)
XLA Modules:
  0.0 25.3 jit_solution(1632973676554027063)
XLA Ops:
  0.0 0.0 copy-start
  0.0 24.6 %shard_map.100 = f32[64,1024]{1,0:T(8,128)S(1)} custom-call(bf16[64,1024]{1,0:T(8,128)(2,1)} %x_hbm.1, s32[1,64]{1,0:T(1,128)} %bitcast.8, s32[2,64]{1,0:T(2,128)} %bitcast.6, f32[1,64]{1,0:T(1,128)} %bitcast.9, f32[2,64]{1,0:T(2,128)} %bitcast.7, f32[1,1024]{1,0:T(1,128)} %bitcast.5, bf16[1,1024,1024]{2,1,0:T(8,128)(2,1)} %wg_hbm.1, ...), custom_call_target="tpu_custom_call" | custom-call | tf_op jit(solution)/shard_map/pallas_call | solution.py:453
  24.6 0.0 copy-done
  24.6 0.7 %multiply_convert_fusion = bf16[64,1024]{1,0:T(8,128)(2,1)} fusion(f32[64,1024]{1,0:T(8,128)S(1)} %shard_map.100, f32[1024]{0:T(1024)S(1)} %copy-done), kind=kLoop, calls=%fused_computation | loop fusion | flops 131072 | bytes 397312 | tf_op jit(solution)/shard_map/convert_element_type | solution.py:503
Async XLA Ops:
  0.0 24.6 %copy-start = (f32[1024]{0:T(1024)S(1)}, f32[1024]{0:T(1024)}, u32[]{:S(2)}) copy-start(f32[1024]{0:T(1024)} %param.19) | copy-start | bytes 12292

commit v4 on v3

--- a/solution.py
+++ b/solution.py
@@ -16,10 +16,10 @@
 BACK = (2, 3, 1)
 AT_ONCE = 2
 EVEN_PLAN = (
-    ("b", 0), ("w", 0), ("f", 0), ("a", 1), ("w", 1), ("b", 1), ("a", 2), ("w", 2), ("b", 2), ("s", 0), ("a", 3), ("w", 3), ("b", 3),
+    ("b", 0), ("w", 0), ("f", 0), ("a", 1), ("w", 1), ("b", 1), ("a", 2), ("w", 2), ("b", 2), ("a", 3), ("w", 3), ("s", 0), ("b", 3),
 )
 ODD_PLAN = (
-    ("b", 0), ("f", 0), ("a", 1), ("a", 2), ("b", 1), ("a", 3), ("s", 0), ("b", 2), ("b", 3),
+    ("w", 2), ("w", 3), ("b", 0), ("f", 0), ("a", 1), ("a", 2), ("b", 1), ("a", 3), ("s", 0), ("b", 2), ("b", 3),
 )
 PLAN = (
     ("s", 1), ("c", 1), ("s", 2), ("c", 2), ("s", 3), ("c", 3), ("c", 0),
@@ -31,7 +31,8 @@
 W_PIECES = 8
 W_CUTS = ((0, 2), (2, 4), (4, 6), (6, 8))
 C_FIRST = 1
-EARLY = 4
+EARLY = 2
+SPLIT = (2,)
 RELAY_SEND = (2, 1)
 RELAY_TAKE = ((2, 1, 3), (1, 2, 3), (2, 1, 3), (2, 3, 1))
 VMEM_LIMIT = 56 * 2**20
@@ -277,23 +278,35 @@
         for j in range(each if relay else 0 if c > 0 else 1, each):
             o, _ = route(take, c, j)
             arrive(xr.at[rows_of(o, 1)], x_recv.at[o - 1, 0])
-        vals = xr[at, :].astype(F32)
-        rows_in = (vals * ngain).astype(BF16)
-        square = jnp.sum(vals * vals, axis=1, keepdims=True)
-        gate = jnp.dot(rows_in, wg[...], preferred_element_type=F32)
-        up = jnp.dot(rows_in, wu[...], preferred_element_type=F32)
-
-        def part(of, whose):
-            return jnp.where(whose == 0, of[:count], of[count:])
-
-        ps[mine(c), pl.ds(0, ff)] = part(gate, 1 - side).astype(BF16)
-        ps[mine(c), pl.ds(ff, ff)] = part(up, 1 - side).astype(BF16)
-        ps[mine(c), tail] = pack(part(square, 1 - side))
-        if c > 0:
-            send(ps.at[mine(c)], pr.at[mine(c)], 1, p_recv.at[c], mate)
-        own[mine(c), pl.ds(0, ff)] = part(gate, side)
-        own[mine(c), pl.ds(ff, ff)] = part(up, side)
-        own[mine(c), tail] = jnp.broadcast_to(part(square, side), (count, LANES))
+        here = mine(c)
+
+        def products(rows):
+            vals = xr[rows, :].astype(F32)
+            rows_in = (vals * ngain).astype(BF16)
+            square = jnp.sum(vals * vals, axis=1, keepdims=True)
+            gate = jnp.dot(rows_in, wg[...], preferred_element_type=F32)
+            return gate, jnp.dot(rows_in, wu[...], preferred_element_type=F32), square
+
+        def hand_over(gate, up, square):
+            ps[here, pl.ds(0, ff)] = gate.astype(BF16)
+            ps[here, pl.ds(ff, ff)] = up.astype(BF16)
+            ps[here, tail] = pack(square)
+            if c > 0:
+                send(ps.at[here], pr.at[here], 1, p_recv.at[c], mate)
+
+        def keep(gate, up, square):
+            own[here, pl.ds(0, ff)] = gate
+            own[here, pl.ds(ff, ff)] = up
+            own[here, tail] = jnp.broadcast_to(square, (count, LANES))
+
+        if c in SPLIT:
+            first = route(take, c, 0)[0] * cap
+            for use, whose in ((hand_over, 1 - side), (keep, side)):
+                use(*products(pl.ds(pl.multiple_of(first + whose * count, count), count)))
+        else:
+            both = products(at)
+            for use, whose in ((hand_over, 1 - side), (keep, side)):
+                use(*(jnp.where(whose == 0, of[:count], of[count:]) for of in both))
 
     def stage_b(c):
         at = mine(c)

time: 25.4 us -> 25.2 us (level)
  no operation moved by 1% of the time
where the time goes in v4:
time: 25.2 us; the launch traced here: 25.1 us
  Pallas kernels  24.4 us (97%)
  other arithmetic  0.67 us (3%)
    pallas_call x1, Pallas kernels, local(): pl.pallas_call(functools.partial(kernel, (n_ep, n_tp, groups)), out_shape...  24.4 us
    convert_element_type x1, other arithmetic, local(): return (normal * final_gain[None, :]).astype(BF16)  0.67 us

profile of v4, /device:TPU:0, one launch (start us, length us, event | category | flops | bytes accessed | tf_op | source)
XLA Modules:
  0.0 25.1 jit_solution(6272976691413488609)
XLA Ops:
  0.0 0.0 copy-start
  0.0 24.4 %shard_map.100 = f32[64,1024]{1,0:T(8,128)S(1)} custom-call(bf16[64,1024]{1,0:T(8,128)(2,1)} %x_hbm.1, s32[1,64]{1,0:T(1,128)} %bitcast.8, s32[2,64]{1,0:T(2,128)} %bitcast.6, f32[1,64]{1,0:T(1,128)} %bitcast.9, f32[2,64]{1,0:T(2,128)} %bitcast.7, f32[1,1024]{1,0:T(1,128)} %bitcast.5, bf16[1,1024,1024]{2,1,0:T(8,128)(2,1)} %wg_hbm.1, ...), custom_call_target="tpu_custom_call" | custom-call | tf_op jit(solution)/shard_map/pallas_call | solution.py:466
  24.4 0.0 copy-done
  24.4 0.7 %multiply_convert_fusion = bf16[64,1024]{1,0:T(8,128)(2,1)} fusion(f32[64,1024]{1,0:T(8,128)S(1)} %shard_map.100, f32[1024]{0:T(1024)S(1)} %copy-done), kind=kLoop, calls=%fused_computation | loop fusion | flops 131072 | bytes 397312 | tf_op jit(solution)/shard_map/convert_element_type | solution.py:516
Async XLA Ops:
  0.0 24.4 %copy-start = (f32[1024]{0:T(1024)S(1)}, f32[1024]{0:T(1024)}, u32[]{:S(2)}) copy-start(f32[1024]{0:T(1024)} %param.19) | copy-start | bytes 12292

commit v5 on v4

--- a/solution.py
+++ b/solution.py
@@ -355,7 +355,7 @@
                     dst[...] = src[...]
 
                 def away():
-                    send(src, dst, 4, o_recv.at[block], {"ep": to, "tp": me_t - odd + q})
+                    send(src, dst, 4, o_recv.at[o], {"ep": to, "tp": me_t - odd + q})
 
                 if c + j > 0:
                     away()
@@ -404,12 +404,10 @@
     for k in [*range(each), *(q * each + j for q in BACK for j in range(each))]:
         block = pl.ds(k * cap, cap)
         if k > 0:
-            for h in range(cap // unit):
-                b = k * (cap // unit) + h
-                arrive(ret.at[pl.ds(b * unit, unit)], o_recv.at[b])
+            arrive(ret.at[block], o_recv.at[k])
         elif each == 1:
             b = 1 - side
-            arrive(ret.at[pl.ds(pl.multiple_of(b * unit, unit), unit)], o_recv.at[b])
+            arrive(ret.at[pl.ds(pl.multiple_of(b * unit, unit), unit)], o_recv.at[0])
         else:
             pl.when(side == 1)(lambda: arrive(ret.at[pl.ds(0, unit)], o_recv.at[0]))
         rows = ret[block, :].astype(F32)
@@ -458,7 +456,6 @@
         ff, top = w_gate.shape[2], member_choice.shape[1]
         cap = tok // groups
         all_rows = n_ep * cap
-        unit = min(cap, all_rows // CHUNKS // 2)
         out_width = -(-tok // 128) * 128
         vmem = pl.BlockSpec(memory_space=pltpu.VMEM)
         hbm = pl.BlockSpec(memory_space=pltpu.HBM)
@@ -497,7 +494,7 @@
                 dma((n_ep - 1, PIECES)),
                 dma((CHUNKS,)),
                 dma((CHUNKS, n_far)),
-                dma((all_rows // unit,)),
+                dma((n_ep,)),
                 dma,
                 dma,
             ],

time: 25.2 us -> 25.2 us (level)
  no operation moved by 1% of the time
where the time goes in v5:
time: 25.2 us; the launch traced here: 25 us
  Pallas kernels  24.4 us (97%)
  other arithmetic  0.67 us (3%)
    pallas_call x1, Pallas kernels, local(): pl.pallas_call(functools.partial(kernel, (n_ep, n_tp, groups)), out_shape...  24.4 us
    convert_element_type x1, other arithmetic, local(): return (normal * final_gain[None, :]).astype(BF16)  0.67 us

profile of v5, /device:TPU:0, one launch (start us, length us, event | category | flops | bytes accessed | tf_op | source)
XLA Modules:
  0.0 25.0 jit_solution(1693367106006461003)
XLA Ops:
  0.0 0.0 copy-start
  0.0 24.4 %shard_map.100 = f32[64,1024]{1,0:T(8,128)S(1)} custom-call(bf16[64,1024]{1,0:T(8,128)(2,1)} %x_hbm.1, s32[1,64]{1,0:T(1,128)} %bitcast.8, s32[2,64]{1,0:T(2,128)} %bitcast.6, f32[1,64]{1,0:T(1,128)} %bitcast.9, f32[2,64]{1,0:T(2,128)} %bitcast.7, f32[1,1024]{1,0:T(1,128)} %bitcast.5, bf16[1,1024,1024]{2,1,0:T(8,128)(2,1)} %wg_hbm.1, ...), custom_call_target="tpu_custom_call" | custom-call | tf_op jit(solution)/shard_map/pallas_call | solution.py:463
  24.4 0.0 copy-done
  24.4 0.7 %multiply_convert_fusion = bf16[64,1024]{1,0:T(8,128)(2,1)} fusion(f32[64,1024]{1,0:T(8,128)S(1)} %shard_map.100, f32[1024]{0:T(1024)S(1)} %copy-done), kind=kLoop, calls=%fused_computation | loop fusion | flops 131072 | bytes 397312 | tf_op jit(solution)/shard_map/convert_element_type | solution.py:513
Async XLA Ops:
  0.0 24.4 %copy-start = (f32[1024]{0:T(1024)S(1)}, f32[1024]{0:T(1024)}, u32[]{:S(2)}) copy-start(f32[1024]{0:T(1024)} %param.19) | copy-start | bytes 12292
